TPU v7x, 32 devices: a whole 2x2x4 slice. The times are simulated.
32 devices in a mesh: grp: 2 (over y), sp: 4 (over z), tp: 4 (over x, core).
Axes of the slice: x: 2, y: 2, z: 4, core: 2. Of those that a mesh axis runs over, the one named last changes fastest.
Arguments:
- query_rows: bfloat16 [3072, 2048], P(('grp', 'sp'), 'tp'), parts along dimension 0, may hold values from -6 to 6, as said below
- key_rows: bfloat16 [3072, 1024], P(('grp', 'sp'), 'tp'), parts along dimension 0, may hold values from -6 to 6, as said below
- value_rows: bfloat16 [3072, 1024], P(('grp', 'sp'), 'tp'), parts along dimension 0, may hold values from -15 to 15
- pool_input: bfloat16 [3072, 2048], P(('grp', 'sp'), 'tp'), parts along dimension 0, may hold values from -6 to 6
- log_gate_sums: float32 [3072, 16], P(('grp', 'sp'), 'tp'), parts along dimension 0, as said below
- query_gain: float32 [128], replicated, may hold values from 0.7 to 4.5, as said below
- key_gain: float32 [128], replicated, may hold values from 0.7 to 4.5, as said below
- pool_weight: bfloat16 [8, 256, 256], P('tp'), may hold values from -0.375 to 0.375
- pool_scale: float32 [2048], P('tp'), may hold values from 0.1 to 1.9
- attention_out: bfloat16 [2048, 4096], P('tp'), may hold values from -0.09375 to 0.09375
- pooling_out: bfloat16 [2048, 4096], P('tp'), may hold values from -0.09375 to 0.09375
Outputs:
- mixed_rows: bfloat16 [3072, 4096], P(('grp', 'sp', 'tp')), parts along dimension 0
There are 2 independent parts, one for each index of `grp`. A program takes and returns all parts, laid end to end along the dimension named above; an argument that names none is the same for every part. Nothing has to cross between parts.
Inputs may be any that keep to these rules, and one draw needn't show every extreme that they name: `query_rows`: normal entries; in some rows a query head's entries may equal its key head's entries of an earlier position. `key_rows`: normal entries. `log_gate_sums`: each column never rises from one position to the next. `query_gain`: Positive. `key_gain`: Positive.
All inputs are finite; a program needn't handle non-finite values.
Results may differ from a plain program's by a relative error of at most 0.014.
The roundings to bfloat16 on the way count: a program that leaves them out, or rounds other values in their place, can miss the bound.
Values may be sent and summed in bfloat16 or wider, within the bound.
A program may use at most 64 MiB of HBM per device.

v0:
```python
import math
import jax
import jax.numpy as jnp
from jax import lax
from jax.sharding import PartitionSpec as P

HEAD = 128
QUERY_HEADS = 16
KV_HEADS = 8
GROUP = 256
MAX_WINDOW = 16
epsilon = 1e-06
masked = -1e30


def from_behind(block, axis, distance):
    devices = range(lax.axis_size(axis))
    route = [(i - distance, i) for i in devices if i - distance in devices]
    return lax.ppermute(block, axis, route)


def head_norm(row_data, gain_vector, head_count):
    shaped = row_data.astype(jnp.float32).reshape(row_data.shape[0], head_count, -1)
    scaled = shaped * lax.rsqrt(jnp.mean(shaped * shaped, axis=-1, keepdims=True) + epsilon)
    return (scaled * gain_vector).astype(jnp.bfloat16)


def window_means(padded, length, first_pos, windows):
    rim_rows = padded.shape[0] - length
    window_sum = jnp.zeros((length,) + padded.shape[1:], jnp.float32)
    pooled = window_sum
    for lookback in range(rim_rows + 1):
        window_sum = window_sum + padded[rim_rows - lookback : rim_rows - lookback + length]
        window_size = lookback + 1
        if window_size >= 2 and window_size & window_size - 1 == 0:
            pooled = jnp.where((windows == window_size)[None, :, None], window_sum, pooled)
    positions = (first_pos + jnp.arange(length, dtype=jnp.int32)).astype(jnp.float32)
    counts = jnp.minimum(positions[:, None, None] + 1.0, windows.astype(jnp.float32)[None, :, None])
    return pooled / counts - padded[rim_rows:]


def attend_block(running, queries, query_gates, query_pos, pair_block, key_gates, key_pos):
    row_best, weight_sum, accumulated = running
    scores = jnp.einsum(
        "tkrd,skd->krts", queries, pair_block[0], preferred_element_type=jnp.float32
    )
    scores = scores * (1.0 / math.sqrt(HEAD)) + query_gates - key_gates
    allowed = key_pos[None, :] <= query_pos[:, None]
    scores = jnp.where(allowed, scores, masked)
    new_best = jnp.maximum(row_best, jnp.max(scores, axis=-1, keepdims=True))
    weights = jnp.where(allowed, jnp.exp(scores - new_best), 0.0)
    fading = jnp.exp(row_best - new_best)
    weight_sum = weight_sum * fading + jnp.sum(weights, axis=-1, keepdims=True)
    summed = jnp.einsum(
        "krts,skd->krtd",
        weights.astype(jnp.bfloat16),
        pair_block[1],
        preferred_element_type=jnp.float32,
    )
    return (new_best, weight_sum, accumulated * fading + summed)


def attend_piece(running, piece, queries, query_gates, query_pos, all_gates, valid):
    kv_here = queries.shape[1]
    ratio = queries.shape[2]
    piece_rows = piece.shape[1]
    block_rows = piece_rows
    while block_rows > 1024 and block_rows % 2 == 0:
        block_rows = block_rows // 2
    last_query = query_pos[query_pos.shape[0] - 1]

    def one_block(block_index, loop_state):
        first = block_index * block_rows

        def compute(state):
            pair_block = lax.dynamic_slice_in_dim(piece, block_index * block_rows, block_rows, 1)
            gate_block = lax.dynamic_slice_in_dim(all_gates, jnp.maximum(first, 0), block_rows, 0)
            gate_block = gate_block.T.reshape(kv_here, ratio, 1, block_rows)
            key_pos = first + jnp.arange(block_rows, dtype=jnp.int32)
            return attend_block(
                state, queries, query_gates, query_pos, pair_block, gate_block, key_pos
            )

        needed = jnp.logical_and(valid, first <= last_query)
        return lax.cond(needed, compute, lambda state: state, loop_state)

    return lax.fori_loop(0, piece_rows // block_rows, one_block, running)


def body(
    query_rows,
    key_rows,
    value_rows,
    pool_input,
    log_gate_sums,
    query_gain,
    key_gain,
    pool_weight,
    pool_scale,
    attention_out,
    pooling_out,
):
    length = query_rows.shape[0]
    kv_here = key_rows.shape[1] // HEAD
    ratio = QUERY_HEADS // KV_HEADS
    sp_index = lax.axis_index("sp")
    queries = head_norm(query_rows, query_gain, kv_here * ratio).reshape(
        length, kv_here, ratio, HEAD
    )
    pair = jnp.stack(
        [head_norm(key_rows, key_gain, kv_here), value_rows.reshape(length, kv_here, HEAD)]
    )
    all_gates = lax.all_gather(log_gate_sums, "sp", axis=0, tiled=True)
    query_gates = log_gate_sums.T.reshape(kv_here, ratio, length, 1)
    query_pos = sp_index * length + jnp.arange(length, dtype=jnp.int32)
    start_state = (
        jnp.full((kv_here, ratio, length, 1), masked, jnp.float32),
        jnp.zeros((kv_here, ratio, length, 1), jnp.float32),
        jnp.zeros((kv_here, ratio, length, HEAD), jnp.float32),
    )
    row_best, weight_sum, accumulated = attend_piece(
        start_state,
        lax.all_gather(pair, "sp", axis=1, tiled=True),
        queries,
        query_gates,
        query_pos,
        all_gates,
        jnp.int32(0) >= 0,
    )
    attended = (
        (accumulated / weight_sum)
        .transpose(2, 0, 1, 3)
        .reshape(length, kv_here * ratio * HEAD)
        .astype(jnp.bfloat16)
    )
    group_here = pool_input.shape[1] // GROUP
    rim = from_behind(pool_input[length - (MAX_WINDOW - 1) :], "sp", 1)
    padded = (
        jnp.concatenate([rim, pool_input])
        .astype(jnp.float32)
        .reshape(length + MAX_WINDOW - 1, group_here, GROUP)
    )
    levels = MAX_WINDOW.bit_length() - 1
    groups = lax.axis_index("tp") * group_here + jnp.arange(group_here, dtype=jnp.int32)
    windows = 2 ** (1 + groups % levels)
    pooled = window_means(padded, length, sp_index * length, windows).astype(jnp.bfloat16)
    mixing = jnp.einsum("tgc,gcd->tgd", pooled, pool_weight, preferred_element_type=jnp.float32)
    pool_mixed = (
        (mixing * pool_scale.reshape(group_here, GROUP))
        .astype(jnp.bfloat16)
        .reshape(length, group_here * GROUP)
    )
    total = jnp.dot(attended, attention_out, preferred_element_type=jnp.float32)
    return lax.psum_scatter(
        (total + jnp.dot(pool_mixed, pooling_out, preferred_element_type=jnp.float32)).astype(
            jnp.bfloat16
        ),
        "tp",
        scatter_dimension=0,
        tiled=True,
    )


def solution(mesh):
    return jax.shard_map(
        body,
        mesh=mesh,
        in_specs=(
            P(("grp", "sp"), "tp"),
            P(("grp", "sp"), "tp"),
            P(("grp", "sp"), "tp"),
            P(("grp", "sp"), "tp"),
            P(("grp", "sp"), "tp"),
            P(),
            P(),
            P("tp", None, None),
            P("tp"),
            P("tp", None),
            P("tp", None),
        ),
        out_specs=P(("grp", "sp", "tp"), None),
        check_vma=False,
    )
```

profile of v0, /device:TPU:0, one launch (start us, length us, event | category | flops | bytes accessed | tf_op | source)
XLA Modules:
  0.0 131.0 jit_solution(2364926939648079398)
XLA Ops:
  6.5 0.0 copy-start
  6.5 0.0 copy-start.3
  6.5 0.0 copy-start.5
  6.5 0.0 all-gather.2.cloned.1.call-start
  6.5 0.8 slice.110
  7.3 4.9 %collective-permute-start = (bf16[15,512]{1,0:T(8,128)(2,1)S(1)}, bf16[15,512]{1,0:T(8,128)(2,1)S(1)}, u32[]{:S(2)}, u32[]{:S(2)}) collective-permute-start(bf16[15,512]{1,0:T(8,128)(2,1)S(1)} %slice.110), channel_id=1, source_target_pairs={{0,4},{4,8},{8,12},{1,5},{5,9},{9,13},{2,6},{6,10},{10,14},{3,7},{... | collective-permute-start | bytes 46088 | tf_op jit(solution)/shard_map/ppermute | solution.py:19
  12.3 1.1 copy.32
  13.4 0.1 bitcast_reduce_fusion.1
  13.5 1.1 copy.33
  14.6 0.8 multiply_convert_fusion.1
  15.3 0.8 pad_maximum_fusion
  16.1 0.0 all-gather.2.cloned.1.call-update
  16.1 0.0 reduce-scatter.2.cloned.1.call-start
  16.2 1.2 copy.34
  17.4 0.1 bitcast_reduce_fusion
  17.6 0.1 broadcast_minimum_fusion
  17.7 0.8 multiply_convert_fusion
  18.5 0.7 mul.203
  19.2 0.6 slice.109
  19.8 0.9 copy.36
  20.7 0.0 copy-done.5
  20.7 13.7 %all_gather.7 = f32[1536,4]{0,1:T(4,128)S(1)} all-gather(f32[384,4]{0,1:T(4,128)S(1)} %copy-done.5), channel_id=1, replica_groups=mesh['grp'=2,'sp'=4,'tp'=4] {'sp'}, dimensions={0}, use_global_device_ids=true | all-gather | bytes 30720 | tf_op jit(solution)/shard_map/all_gather | solution.py:113
  34.4 0.0 collective-permute-done
  34.4 0.0 copy-done.3
  34.4 0.1 maximum_convert_fusion
  34.5 3.6 %fusion.30 = (f32[384,512]{1,0:T(8,128)S(1)}, f32[384,512]{1,0:T(8,128)S(1)}, f32[384,512]{1,0:T(8,128)S(1)}, f32[384,512]{1,0:T(8,128)S(1)}, f32[384,512]{1,0:T...) fusion(f32[399,512]{1,0:T(8,128)S(1)} %maximum_convert_fusion), kind=kLoop, calls=%fused_computation.80 | loop fusion | bytes 25165824 | tf_op jit(solution)/shard_map/slice | solution.py:33
  38.1 0.0 copy-done
  38.1 0.0 copy-start.4
  38.1 4.8 %fusion.20 = bf16[2,384,256]{1,2,0:T(8,128)(2,1)S(1)} fusion(bf16[2,256,256]{2,1,0:T(8,128)(2,1)S(1)} %copy-done, f32[2,256]{1,0:T(2,128)S(1)} %mul.203, f32[48,2,8,256]{3,2,1,0:T(8,128)S(1)} %bitcast.209, f32[48,2,8,256]{3,2,1,0:T(8,128)S(1)} %bitcast.210, f32[48,2,8,256]{3,2,1,0:T(8,128)S(1)} %bitcast.211, f32[48,2,8,256]{3,2,1,0:T(8,128)S(1)} %bitcast.212, ...), kind=kOutput, calls=%fused_computation.29 | convolution fusion | flops 105381888 | bytes 13243400 | tf_op jit(solution)/shard_map/tgc,gcd->tgd/dot_general | solution.py:147
  42.9 10.5 %all-gather.2.cloned.1.call-done = bf16[2,1536,2,128]{1,3,2,0:T(8,128)(2,1)} async-done(((bf16[2,384,2,128]{1,3,2,0:T(8,128)(2,1)}), bf16[2,1536,2,128]{1,3,2,0:T(8,128)(2,1)}) %all-gather.2.cloned.1.call-update) | async-done | bytes 1572880 | tf_op jit(solution)/shard_map/all_gather | solution.py:123
  53.3 2.6 %copy.35 = bf16[2,1536,2,128]{3,1,2,0:T(8,128)(2,1)} copy(bf16[2,1536,2,128]{1,3,2,0:T(8,128)(2,1)} %all-gather.2.cloned.1.call-done) | data formatting | bytes 3145728
  55.9 0.1 broadcast_in_dim.71
  56.0 0.0 copy-done.4
  56.0 11.9 %while.18 = (s32[]{:T(128)}, f32[2,2,384,1]{2,1,0,3:T(2,128)S(1)}, f32[2,2,384,1]{2,1,0,3:T(2,128)S(1)}, f32[2,2,384,128]{3,2,1,0:T(8,128)S(1)}, s32[]{:T(128)},...) while((s32[]{:T(128)}, f32[2,2,384,1]{2,1,0,3:T(2,128)S(1)}, ...), condition=%wide.region_7.8_spmd.clone, body=%wide.region_2.7_spmd.clone.sunk | while | flops 627086976 | bytes 37177752 | solution.py:87
  56.6 10.6 %conditional.3 = ((f32[2,2,384,1]{2,1,0,3:T(2,128)S(1)}, f32[2,2,384,1]{2,1,0,3:T(2,128)S(1)}, f32[2,2,384,128]{3,2,1,0:T(8,128)S(1)})) conditional(s32[]{:T(128)} %convert_element_type.104, (f32[2,2,384,1]{2,1,0,3:T(2,128)S(1)}, f32[2,2,384,1]{2,1,0,3:T(2,128)S(1)}, f32[2,2,384,128]{3,2,1,0:T(8,128)S(1)}) %tuple.62, (s32[]{:T(128)}, s32[]{:T(128)}, ...), branch_computations={%region_3.0_spmd, %region_4.6_spmd} | conditional | flops 627086976 | bytes 37175960 | solution.py:85
  56.7 0.2 broadcast_compare_fusion
  56.9 0.1 dynamic-slice_bitcast_fusion.4
  57.0 3.9 %fusion.6 = (f32[2,2,384]{2,1,0:T(2,128)S(1)}, f32[2,768,384,2]{2,1,3,0:T(8,128)}) fusion(f32[2,2,768]{2,1,0:T(2,128)S(1)} %sub.6, f32[2,2,384]{2,1,0:T(2,128)S(1)} %bitcast.231, pred[384,768]{0,1:T(8,128)(4,1)S(1)} %broadcast_compare_fusion, bf16[384,2,2,128]{3,0,2,1:T(8,128)(2,1)S(1)} %get-tuple-element.199, ...), kind=kOutput, calls=%fused_computation.7 | convolution fusion | flops 307886592 | bytes 5824516 | tf_op jit(solution)/shard_map/while/body/eval_jaxpr/cond/branch_1_fun/tkrd,skd->krts/dot_general | solution.py:44
  60.9 0.0 copy-start.1
  61.0 4.6 %fusion.10 = f32[2,2,384,128]{3,2,1,0:T(8,128)S(1)} fusion(f32[2,768,384,2]{2,1,3,0:T(8,128)} %get-tuple-element.284, f32[2,2,384]{2,1,0:T(2,128)S(1)} %bitcast.224, f32[2,2,768]{2,1,0:T(2,128)S(1)} %sub.6, f32[2,2,384]{2,1,0:T(2,128)S(1)} %bitcast.232, pred[384,768]{0,1:T(8,128)(4,1)S(1)} %broadcast_compare_fusion, ...), kind=kOutput, calls=%fused_computation.10 | convolution fusion | flops 310640640 | bytes 7010312 | tf_op jit(solution)/shard_map/while/body/eval_jaxpr/cond/branch_1_fun/krts,skd->krtd/dot_general | solution.py:54
  65.6 0.0 copy-done.1
  65.6 1.6 %fusion.5 = f32[2,2,384]{2,1,0:T(2,128)S(1)} fusion(f32[2,768,384,2]{2,1,3,0:T(8,128)S(1)} %copy-done.1, f32[2,2,384]{2,1,0:T(2,128)S(1)} %bitcast.225, f32[2,2,768]{2,1,0:T(2,128)S(1)} %sub.6, f32[2,2,384]{2,1,0:T(2,128)S(1)} %bitcast.233, pred[384,768]{0,1:T(8,128)(4,1)S(1)} %broadcast_compare_fusion), kind=kLoop, calls=%fused_computation.6 | loop fusion | flops 8256000 | bytes 5044224 | tf_op jit(solution)/shard_map/while/body/eval_jaxpr/cond/branch_1_fun/reduce_sum | solution.py:53
  67.9 0.3 copy.37
  68.2 0.1 divide_convert_fusion
  68.2 0.0 copy-start.2
  68.2 4.2 %fusion.31 = f32[384,4096]{1,0:T(8,128)S(1)} fusion(bf16[384,512]{0,1:T(8,128)(2,1)S(1)} %bitcast.228, bf16[512,4096]{1,0:T(8,128)(2,1)} %param.24), kind=kOutput, calls=%fused_computation.81 | convolution fusion | flops 1610612736 | bytes 10878976 | tf_op jit(solution)/shard_map/dot_general | solution.py:153
  72.5 0.0 copy-done.2
  72.5 3.7 %add_convert_fusion = bf16[384,4096]{1,0:T(8,128)(2,1)} fusion(f32[384,4096]{1,0:T(8,128)S(1)} %fusion.31, bf16[384,512]{0,1:T(8,128)(2,1)S(1)} %bitcast.227, bf16[512,4096]{1,0:T(8,128)(2,1)S(1)} %copy-done.2), kind=kOutput, calls=%fused_computation.27 | convolution fusion | flops 1613758464 | bytes 14024704 | tf_op jit(solution)/shard_map/dot_general | solution.py:155
  76.2 0.0 reduce-scatter.2.cloned.1.call-update
  76.2 48.0 %reduce-scatter.2.cloned.1.call-done = bf16[96,4096]{1,0:T(8,128)(2,1)} async-done(((bf16[384,4096]{1,0:T(8,128)(2,1)}), bf16[96,4096]{1,0:T(8,128)(2,1)}) %reduce-scatter.2.cloned.1.call-update) | async-done | bytes 786448 | tf_op jit(solution)/shard_map/reduce_scatter | solution.py:154
  (20 shorter events, 0.2 us)
Async XLA Ops:
  6.5 31.6 %copy-start = (bf16[2,256,256]{2,1,0:T(8,128)(2,1)S(1)}, bf16[2,256,256]{2,1,0:T(8,128)(2,1)}, u32[]{:S(2)}) copy-start(bf16[2,256,256]{2,1,0:T(8,128)(2,1)} %param.22) | copy-start | bytes 786436
  6.5 27.9 %copy-start.3 = (bf16[384,512]{1,0:T(8,128)(2,1)S(1)}, bf16[384,512]{1,0:T(8,128)(2,1)}, u32[]{:S(2)}) copy-start(bf16[384,512]{1,0:T(8,128)(2,1)} %param.18) | copy-start | bytes 1179652
  6.5 14.2 %copy-start.5 = (f32[384,4]{0,1:T(4,128)S(1)}, f32[384,4]{0,1:T(4,128)}, u32[]{:S(2)}) copy-start(f32[384,4]{0,1:T(4,128)} %param.19) | copy-start | bytes 18436
  6.5 46.8 %all-gather.2.cloned.1.call-start = ((), (), s32[]{:S(2)}) async-start(), calls=%async_computation.1 | async-start | bytes 1966080 | tf_op jit(solution)/shard_map/all_gather | solution.py:123
  7.3 27.1 %collective-permute-start = (bf16[15,512]{1,0:T(8,128)(2,1)S(1)}, bf16[15,512]{1,0:T(8,128)(2,1)S(1)}, u32[]{:S(2)}, u32[]{:S(2)}) collective-permute-start(bf16[15,512]{1,0:T(8,128)(2,1)S(1)} %slice.110), channel_id=1, source_target_pairs={{0,4},{4,8},{8,12},{1,5},{5,9},{9,13},{2,6},{6,10},{10,14},{3,7},{... | collective-permute-start | bytes 46088 | tf_op jit(solution)/shard_map/ppermute | solution.py:19
  16.1 108.1 %reduce-scatter.2.cloned.1.call-start = ((), (), s32[]{:S(2)}) async-start(), calls=%async_computation.2 | async-start | bytes 3932160 | tf_op jit(solution)/shard_map/reduce_scatter | solution.py:154
  38.1 17.9 %copy-start.4 = (bf16[384,2,2,128]{3,0,2,1:T(8,128)(2,1)S(1)}, bf16[384,2,2,128]{3,0,2,1:T(8,128)(2,1)}, u32[]{:S(2)}) copy-start(bf16[384,2,2,128]{3,0,2,1:T(8,128)(2,1)} %copy.36) | copy-start | bytes 1179652
  60.9 4.6 %copy-start.1 = (f32[2,768,384,2]{2,1,3,0:T(8,128)S(1)}, f32[2,768,384,2]{2,1,3,0:T(8,128)}, u32[]{:S(2)}) copy-start(f32[2,768,384,2]{2,1,3,0:T(8,128)} %get-tuple-element.284) | copy-start | bytes 14155780 | tf_op jit(solution)/shard_map/while/body/eval_jaxpr/cond
  68.2 4.3 %copy-start.2 = (bf16[512,4096]{1,0:T(8,128)(2,1)S(1)}, bf16[512,4096]{1,0:T(8,128)(2,1)}, u32[]{:S(2)}) copy-start(bf16[512,4096]{1,0:T(8,128)(2,1)} %param.25) | copy-start | bytes 12582916
Sparse Core Ops, SparseCore 0:
  16.3 37.0 all-gather.1
  76.3 47.8 reduce-scatter.1
where the time goes:
time: 131 us
  waiting for transfers between devices  58.5 us (45%)
  matrix products  21.2 us (16%)
  blocking collectives  13.7 us (10%)
  between operations  13.6 us (10%)
  local copies, waits for them, and re-layouts  13 us (10%)
  starting transfers between devices  4.99 us (4%)
  other arithmetic  4.75 us (4%)
  loops' own time  1.31 us (1%)
    reduce_scatter x1, waiting for transfers between devices, body(): lax.psum_scatter((total + jnp.dot(pool_mixed, pooling_out, preferred_elem...  48 us
    all_gather x1, blocking collectives, body(): all_gates = lax.all_gather(log_gate_sums, 'sp', axis=0, tiled=True)  13.7 us
    all_gather x1, waiting for transfers between devices, body(): lax.all_gather(pair, 'sp', axis=1, tiled=True)  10.5 us
    unnamed x15, local copies, waits for them, and re-layouts  6.93 us
    ppermute x1, starting transfers between devices, from_behind(): return lax.ppermute(block, axis, route)  4.94 us
    dot_general x1, matrix products, body(): jnp.einsum('tgc,gcd->tgd', pooled, pool_weight, preferred_element_type=jn...  4.77 us
    dot_general x1, matrix products, attend_block(): jnp.einsum('krts,skd->krtd', weights.astype(jnp.bfloat16), pair_block[1],...  4.59 us
    dot_general x1, matrix products, body(): total = jnp.dot(attended, attention_out, preferred_element_type=jnp.float32)  4.24 us
  transfers between devices with their start and end apart: 3, of which 2 were waited for; matrix products, arithmetic and copies ran while one was open for 13% of the time, Pallas kernels for 0%

commit v1 on v0

--- a/solution.py
+++ b/solution.py
@@ -120,7 +120,9 @@
     )
     row_best, weight_sum, accumulated = attend_piece(
         start_state,
-        lax.all_gather(pair, "sp", axis=1, tiled=True),
+        jnp.concatenate(
+            jax.lax.all_to_all(jnp.stack([pair] * jax.lax.axis_size("sp")), "sp", 0, 0), 1
+        ),
         queries,
         query_gates,
         query_pos,

time: 131 us -> 153 us (1.17)
  blocking collectives: 13.7 us -> 39.9 us
  waiting for transfers between devices: 58.5 us -> 48.9 us
  starting transfers between devices: 4.99 us -> 8.81 us
    all_gather x1, blocking collectives: 13.7 us -> 39.9 us  [body(): all_gates = lax.all_gather(log_gate_sums, 'sp', axis=0, tiled=True)]
    all_gather x1 -> x0, waiting for transfers between devices: 10.5 us -> none  [body(): lax.all_gather(pair, 'sp', axis=1, tiled=True)]
    unnamed x15 -> x16, local copies, waits for them, and re-layouts: 6.93 us -> 1.19 us
    all_to_all x0 -> x1, starting transfers between devices: none -> 3.86 us  [body(): jax.lax.all_to_all(jnp.stack([pair] * jax.lax.axis_size('sp')), 'sp', 0, 0)]
    another operation x0 -> x3, local copies, waits for them, and re-layouts: none -> 2.48 us  [the longest x1 1.46 us: body(): jnp.stack([pair] * jax.lax.axis_size('sp'))]
  transfers between devices with their start and end apart: 3 -> 3, of which waited for: 2 -> 1; matrix products, arithmetic and copies ran while one was open for 13% -> 12% of each run, Pallas kernels for 0% -> 0%
where the time goes in v1:
time: 153 us; the launch traced here: 152 us
  waiting for transfers between devices  48.9 us (32%)
  blocking collectives  39.9 us (26%)
  matrix products  21.6 us (14%)
  between operations  13.7 us (9%)
  local copies, waits for them, and re-layouts  12.2 us (8%)
  starting transfers between devices  8.81 us (6%)
  other arithmetic  5.78 us (4%)
    reduce_scatter x1, waiting for transfers between devices, body(): lax.psum_scatter((total + jnp.dot(pool_mixed, pooling_out, preferred_elem...  48.9 us
    all_gather x1, blocking collectives, body(): all_gates = lax.all_gather(log_gate_sums, 'sp', axis=0, tiled=True)  39.9 us
    dot_general x1, matrix products, body(): jnp.einsum('tgc,gcd->tgd', pooled, pool_weight, preferred_element_type=jn...  5.09 us
    ppermute x1, starting transfers between devices, from_behind(): return lax.ppermute(block, axis, route)  4.94 us
    dot_general x1, matrix products, attend_block(): jnp.einsum('krts,skd->krtd', weights.astype(jnp.bfloat16), pair_block[1],...  4.6 us
    dot_general x1, matrix products, body(): total = jnp.dot(attended, attention_out, preferred_element_type=jnp.float32)  4.23 us
    slice x1, local copies, waits for them, and re-layouts, window_means(): padded[rim_rows - lookback:rim_rows - lookback + length]  3.98 us
    dot_general x1, matrix products, attend_block(): jnp.einsum('tkrd,skd->krts', queries, pair_block[0], preferred_element_ty...  3.96 us
  transfers between devices with their start and end apart: 3, of which 1 were waited for; matrix products, arithmetic and copies ran while one was open for 12% of the time, Pallas kernels for 0%

profile of v1, /device:TPU:0, one launch (start us, length us, event | category | flops | bytes accessed | tf_op | source)
XLA Modules:
  0.0 152.3 jit_solution(9594187118769713685)
XLA Ops:
  6.5 0.0 copy-start
  6.5 0.8 slice.110
  7.3 4.9 %collective-permute-start = (bf16[15,512]{1,0:T(8,128)(2,1)S(1)}, bf16[15,512]{1,0:T(8,128)(2,1)S(1)}, u32[]{:S(2)}, u32[]{:S(2)}) collective-permute-start(bf16[15,512]{1,0:T(8,128)(2,1)S(1)} %slice.110), channel_id=1, source_target_pairs={{0,4},{4,8},{8,12},{1,5},{5,9},{9,13},{2,6},{6,10},{10,14},{3,7},{... | collective-permute-start | bytes 46088 | tf_op jit(solution)/shard_map/ppermute | solution.py:19
  12.3 1.0 convert_multiply_fusion.1
  13.2 0.0 copy-start.3
  13.2 1.2 reshape.188
  14.4 0.2 mul.187
  14.6 0.0 copy-start.7
  14.6 0.5 reduce_sum.27
  15.1 0.0 copy-start.6
  15.1 0.1 copy.131
  15.2 1.0 stack_reshape.3
  16.3 0.0 copy-start.5
  16.3 0.8 fusion.26
  17.2 1.5 stack.5
  18.6 3.9 %all-to-all-start = ((bf16[4,2,384,2,128]{4,2,3,1,0:T(8,128)(2,1)}), bf16[4,2,384,2,128]{4,2,3,1,0:T(8,128)(2,1)S(1)}, u32[]{:S(2)}, u32[]{:S(2)}) async-start(bf16[4,2,384,2,128]{4,2,3,1,0:T(8,128)(2,1)} %stack.5), calls=%async_computation | async-start | bytes 3145728 | tf_op jit(solution)/shard_map/all_to_all | solution.py:124
  22.5 0.0 reduce-scatter.2.cloned.1.call-start
  22.5 0.0 copy-done.3
  22.5 0.2 copy.135
  22.7 0.1 bitcast_reduce_fusion
  22.9 0.1 broadcast_minimum_fusion
  23.0 0.0 copy-done.7
  23.0 0.1 multiply_convert_fusion
  23.1 0.0 copy-done.6
  23.2 0.6 slice.109
  23.8 0.9 copy.136
  24.7 0.0 copy-done.5
  24.7 39.9 %all_gather.3 = f32[1536,4]{0,1:T(4,128)S(1)} all-gather(f32[384,4]{0,1:T(4,128)S(1)} %copy-done.5), channel_id=1, replica_groups=mesh['grp'=2,'sp'=4,'tp'=4] {'sp'}, dimensions={0}, use_global_device_ids=true | all-gather | bytes 30720 | tf_op jit(solution)/shard_map/all_gather | solution.py:113
  64.6 0.0 collective-permute-done
  64.6 1.1 maximum_convert_fusion
  65.7 4.0 %fusion.32 = (f32[384,512]{1,0:T(8,128)S(1)}, f32[384,512]{1,0:T(8,128)S(1)}, f32[384,512]{1,0:T(8,128)S(1)}, f32[384,512]{1,0:T(8,128)}, f32[384,512]{1,0:T(8,1...) fusion(f32[399,512]{1,0:T(8,128)S(1)} %maximum_convert_fusion), kind=kLoop, calls=%fused_computation.81 | loop fusion | bytes 25165824 | tf_op jit(solution)/shard_map/slice | solution.py:33
  69.7 0.0 copy-done
  69.7 0.0 copy-start.4
  69.7 5.1 %fusion.20 = bf16[2,384,256]{1,2,0:T(8,128)(2,1)S(1)} fusion(bf16[2,256,256]{2,1,0:T(8,128)(2,1)S(1)} %copy-done, f32[2,256]{1,0:T(2,128)S(1)} %mul.203, f32[48,2,8,256]{3,2,1,0:T(8,128)S(1)} %bitcast.207, f32[48,2,8,256]{3,2,1,0:T(8,128)S(1)} %bitcast.208, f32[48,2,8,256]{3,2,1,0:T(8,128)} %bitcast.209, f32[48,2,8,256]{3,2,1,0:T(8,128)} %bitcast.210, ...), kind=kOutput, calls=%fused_computation.29 | convolution fusion | flops 105381888 | bytes 13243400 | tf_op jit(solution)/shard_map/tgc,gcd->tgd/dot_general | solution.py:149
  74.8 0.0 all-to-all-done
  74.8 1.3 copy.134
  76.1 0.1 broadcast_in_dim.71
  76.2 0.0 copy-done.4
  76.2 12.0 %while.18 = (s32[]{:T(128)}, f32[2,2,384,1]{2,1,0,3:T(2,128)S(1)}, f32[2,2,384,1]{2,1,0,3:T(2,128)S(1)}, f32[2,2,384,128]{3,2,1,0:T(8,128)S(1)}, s32[]{:T(128)},...) while((s32[]{:T(128)}, f32[2,2,384,1]{2,1,0,3:T(2,128)S(1)}, ...), condition=%wide.region_7.8_spmd.clone, body=%wide.region_2.7_spmd.clone.sunk | while | flops 627086976 | bytes 37177752 | solution.py:87
  76.8 10.7 %conditional.3 = ((f32[2,2,384,1]{2,1,0,3:T(2,128)S(1)}, f32[2,2,384,1]{2,1,0,3:T(2,128)S(1)}, f32[2,2,384,128]{3,2,1,0:T(8,128)S(1)})) conditional(s32[]{:T(128)} %convert_element_type.102, (f32[2,2,384,1]{2,1,0,3:T(2,128)S(1)}, f32[2,2,384,1]{2,1,0,3:T(2,128)S(1)}, f32[2,2,384,128]{3,2,1,0:T(8,128)S(1)}) %tuple.66, (s32[]{:T(128)}, s32[]{:T(128)}, ...), branch_computations={%region_3.0_spmd, %region_4.6_spmd} | conditional | flops 627086976 | bytes 37175960 | solution.py:85
  76.9 0.2 broadcast_compare_fusion
  77.1 0.1 dynamic-slice_bitcast_fusion.4
  77.2 4.0 %fusion.6 = (f32[2,2,384]{2,1,0:T(2,128)S(1)}, f32[2,768,384,2]{2,1,3,0:T(8,128)}) fusion(f32[2,2,768]{2,1,0:T(2,128)S(1)} %sub.6, f32[2,2,384]{2,1,0:T(2,128)S(1)} %bitcast.228, pred[384,768]{0,1:T(8,128)(4,1)S(1)} %broadcast_compare_fusion, bf16[384,2,2,128]{3,0,2,1:T(8,128)(2,1)S(1)} %get-tuple-element.199, ...), kind=kOutput, calls=%fused_computation.7 | convolution fusion | flops 307886592 | bytes 5824516 | tf_op jit(solution)/shard_map/while/body/eval_jaxpr/cond/branch_1_fun/tkrd,skd->krts/dot_general | solution.py:44
  81.2 0.0 copy-start.1
  81.2 4.6 %fusion.10 = f32[2,2,384,128]{3,2,1,0:T(8,128)S(1)} fusion(f32[2,768,384,2]{2,1,3,0:T(8,128)} %get-tuple-element.324, f32[2,2,384]{2,1,0:T(2,128)S(1)} %bitcast.222, f32[2,2,768]{2,1,0:T(2,128)S(1)} %sub.6, f32[2,2,384]{2,1,0:T(2,128)S(1)} %bitcast.229, pred[384,768]{0,1:T(8,128)(4,1)S(1)} %broadcast_compare_fusion, ...), kind=kOutput, calls=%fused_computation.10 | convolution fusion | flops 310640640 | bytes 7010312 | tf_op jit(solution)/shard_map/while/body/eval_jaxpr/cond/branch_1_fun/krts,skd->krtd/dot_general | solution.py:54
  85.8 0.0 copy-done.1
  85.8 1.7 %fusion.5 = f32[2,2,384]{2,1,0:T(2,128)S(1)} fusion(f32[2,768,384,2]{2,1,3,0:T(8,128)S(1)} %copy-done.1, f32[2,2,384]{2,1,0:T(2,128)S(1)} %bitcast.223, f32[2,2,768]{2,1,0:T(2,128)S(1)} %sub.6, f32[2,2,384]{2,1,0:T(2,128)S(1)} %bitcast.230, pred[384,768]{0,1:T(8,128)(4,1)S(1)} %broadcast_compare_fusion), kind=kLoop, calls=%fused_computation.6 | loop fusion | flops 8256000 | bytes 5044224 | tf_op jit(solution)/shard_map/while/body/eval_jaxpr/cond/branch_1_fun/reduce_sum | solution.py:53
  88.2 0.3 copy.137
  88.5 0.1 divide_convert_fusion
  88.6 0.0 copy-start.2
  88.6 4.2 %fusion.33 = f32[384,4096]{1,0:T(8,128)S(1)} fusion(bf16[384,512]{0,1:T(8,128)(2,1)S(1)} %bitcast.226, bf16[512,4096]{1,0:T(8,128)(2,1)} %param.24), kind=kOutput, calls=%fused_computation.82 | convolution fusion | flops 1610612736 | bytes 10878976 | tf_op jit(solution)/shard_map/dot_general | solution.py:155
  92.8 0.0 copy-done.2
  92.8 3.7 %add_convert_fusion = bf16[384,4096]{1,0:T(8,128)(2,1)} fusion(f32[384,4096]{1,0:T(8,128)S(1)} %fusion.33, bf16[384,512]{0,1:T(8,128)(2,1)S(1)} %bitcast.224, bf16[512,4096]{1,0:T(8,128)(2,1)S(1)} %copy-done.2), kind=kOutput, calls=%fused_computation.27 | convolution fusion | flops 1613758464 | bytes 14024704 | tf_op jit(solution)/shard_map/dot_general | solution.py:157
  96.5 0.0 reduce-scatter.2.cloned.1.call-update
  96.5 48.9 %reduce-scatter.2.cloned.1.call-done = bf16[96,4096]{1,0:T(8,128)(2,1)} async-done(((bf16[384,4096]{1,0:T(8,128)(2,1)}), bf16[96,4096]{1,0:T(8,128)(2,1)}) %reduce-scatter.2.cloned.1.call-update) | async-done | bytes 786448 | tf_op jit(solution)/shard_map/reduce_scatter | solution.py:156
  (23 shorter events, 0.3 us)
Async XLA Ops:
  6.5 63.2 %copy-start = (bf16[2,256,256]{2,1,0:T(8,128)(2,1)S(1)}, bf16[2,256,256]{2,1,0:T(8,128)(2,1)}, u32[]{:S(2)}) copy-start(bf16[2,256,256]{2,1,0:T(8,128)(2,1)} %param.22) | copy-start | bytes 786436
  7.3 57.3 %collective-permute-start = (bf16[15,512]{1,0:T(8,128)(2,1)S(1)}, bf16[15,512]{1,0:T(8,128)(2,1)S(1)}, u32[]{:S(2)}, u32[]{:S(2)}) collective-permute-start(bf16[15,512]{1,0:T(8,128)(2,1)S(1)} %slice.110), channel_id=1, source_target_pairs={{0,4},{4,8},{8,12},{1,5},{5,9},{9,13},{2,6},{6,10},{10,14},{3,7},{... | collective-permute-start | bytes 46088 | tf_op jit(solution)/shard_map/ppermute | solution.py:19
  13.2 9.3 %copy-start.3 = (bf16[384,512]{1,0:T(8,128)(2,1)S(1)}, bf16[384,512]{1,0:T(8,128)(2,1)}, u32[]{:S(2)}) copy-start(bf16[384,512]{1,0:T(8,128)(2,1)} %param.15) | copy-start | bytes 1179652
  14.6 8.4 %copy-start.7 = (f32[128]{0:T(128)S(1)}, f32[128]{0:T(128)}, u32[]{:S(2)}) copy-start(f32[128]{0:T(128)} %param.20) | copy-start | bytes 1540
  15.1 8.0 %copy-start.6 = (f32[512]{0:T(512)S(1)}, f32[512]{0:T(512)}, u32[]{:S(2)}) copy-start(f32[512]{0:T(512)} %param.23) | copy-start | bytes 6148
  16.3 8.5 %copy-start.5 = (f32[384,4]{0,1:T(4,128)S(1)}, f32[384,4]{0,1:T(4,128)}, u32[]{:S(2)}) copy-start(f32[384,4]{0,1:T(4,128)} %param.19) | copy-start | bytes 18436
  18.6 56.2 %all-to-all-start = ((bf16[4,2,384,2,128]{4,2,3,1,0:T(8,128)(2,1)}), bf16[4,2,384,2,128]{4,2,3,1,0:T(8,128)(2,1)S(1)}, u32[]{:S(2)}, u32[]{:S(2)}) async-start(bf16[4,2,384,2,128]{4,2,3,1,0:T(8,128)(2,1)} %stack.5), calls=%async_computation | async-start | bytes 3145728 | tf_op jit(solution)/shard_map/all_to_all | solution.py:124
  22.5 123.0 %reduce-scatter.2.cloned.1.call-start = ((), (), s32[]{:S(2)}) async-start(), calls=%async_computation.2 | async-start | bytes 3932160 | tf_op jit(solution)/shard_map/reduce_scatter | solution.py:156
  69.7 6.5 %copy-start.4 = (bf16[384,2,2,128]{3,0,2,1:T(8,128)(2,1)S(1)}, bf16[384,2,2,128]{3,0,2,1:T(8,128)(2,1)}, u32[]{:S(2)}) copy-start(bf16[384,2,2,128]{3,0,2,1:T(8,128)(2,1)} %copy.136) | copy-start | bytes 1179652
  81.2 4.6 %copy-start.1 = (f32[2,768,384,2]{2,1,3,0:T(8,128)S(1)}, f32[2,768,384,2]{2,1,3,0:T(8,128)}, u32[]{:S(2)}) copy-start(f32[2,768,384,2]{2,1,3,0:T(8,128)} %get-tuple-element.324) | copy-start | bytes 14155780 | tf_op jit(solution)/shard_map/while/body/eval_jaxpr/cond
  88.6 4.2 %copy-start.2 = (bf16[512,4096]{1,0:T(8,128)(2,1)S(1)}, bf16[512,4096]{1,0:T(8,128)(2,1)}, u32[]{:S(2)}) copy-start(bf16[512,4096]{1,0:T(8,128)(2,1)} %param.25) | copy-start | bytes 12582916
Sparse Core Ops, SparseCore 0:
  96.7 48.7 reduce-scatter.1
